TPU v7x, 32 devices: a whole 2x2x4 slice. The times are simulated.
32 devices in a mesh: ep: 8 (over z, x), tp: 4 (over y, core).
Axes of the slice: x: 2, y: 2, z: 4, core: 2. Of those that a mesh axis runs over, the one named last changes fastest.
Arguments:
- tokens: bfloat16 [128, 1024], P('ep'), may hold values from -6 to 6
- norm_gain: float32 [1024], replicated, may hold values from 0.1 to 1.9
- routing: int32 [128, 2], P('ep'), may hold values from 0 to 7, all different within a row; in each aligned block of 16 rows (0 to 15, 16 to 31, ...) at most 8 rows name the same one
- route_weight: float32 [128, 2], P('ep'), may hold values from 0.1 to 1
- w_gate: bfloat16 [8, 1024, 3584], P('ep', None, 'tp'), may hold values from -0.1875 to 0.1875
- w_up: bfloat16 [8, 1024, 3584], P('ep', None, 'tp'), may hold values from -0.1875 to 0.1875
- w_down: bfloat16 [8, 3584, 1024], P('ep', 'tp'), may hold values from -0.09375 to 0.09375
Outputs:
- mixed: bfloat16 [128, 1024], P('ep', 'tp')
Inputs may be any that keep to these rules, and one draw needn't show every extreme that they name: `routing`: each row names 2 different experts of 0 to 7; among the 16 tokens of one index of ep no expert is named more than 8 times, and in some draws' blocks exactly 8 times.
All inputs are finite; a program needn't handle non-finite values.
Results may differ from a plain program's by a relative error of at most 0.0022.
Values may be sent and summed in bfloat16 or wider, within the bound.
A program may use at most 64 MiB of HBM per device.

v0:
```python
import jax
import jax.numpy as jnp
from jax import lax
from jax.sharding import PartitionSpec as P

CAP = 8


norm_eps = 1e-06


def local(tokens, norm_gain, routing, route_weight, w_gate, w_up, w_down):
    token_count = tokens.shape[0]
    top_count = routing.shape[1]
    width = tokens.shape[1]
    local_experts = w_gate.shape[0]
    groups = lax.axis_size("ep")
    experts = local_experts * groups
    values = tokens.astype(jnp.float32)
    scale = lax.rsqrt(jnp.mean(values * values, axis=-1, keepdims=True) + norm_eps)
    normed = (values * scale * norm_gain).astype(jnp.bfloat16)
    flat_ids = routing.reshape(-1)
    one_hot = (flat_ids[:, None] == jnp.arange(experts, dtype=jnp.int32)[None, :]).astype(jnp.int32)
    before = jnp.cumsum(one_hot, axis=0) - one_hot
    slot_index = jnp.sum(before * one_hot, axis=1)
    position = flat_ids * CAP + slot_index
    placing = jnp.arange(experts * CAP, dtype=jnp.int32)[:, None] == position[None, :]
    token_rows = jnp.repeat(normed, top_count, axis=0)
    outgoing = jnp.dot(placing.astype(jnp.bfloat16), token_rows, preferred_element_type=jnp.float32)
    outgoing = outgoing.astype(jnp.bfloat16).reshape(experts, CAP, width)
    incoming = lax.all_to_all(outgoing, "ep", split_axis=0, concat_axis=0, tiled=True)
    incoming = incoming.reshape(groups, local_experts, CAP, width)
    gate_act = jnp.einsum("secd,edf->secf", incoming, w_gate, preferred_element_type=jnp.float32)
    up_act = jnp.einsum("secd,edf->secf", incoming, w_up, preferred_element_type=jnp.float32)
    hidden = (jax.nn.silu(gate_act) * up_act).astype(jnp.bfloat16)
    partial_out = jnp.einsum("secf,efd->secd", hidden, w_down, preferred_element_type=jnp.float32)
    partial_out = partial_out.reshape(experts, CAP, width)
    weighted = jnp.where(placing.T, route_weight.reshape(-1)[:, None], 0.0)
    weighted = jnp.sum(weighted.reshape(token_count, top_count, experts * CAP), axis=1)
    summed = lax.psum_scatter(partial_out, "tp", scatter_dimension=2, tiled=True)
    arrived = lax.all_to_all(summed, "ep", split_axis=0, concat_axis=0, tiled=True)
    mixed = jnp.dot(weighted, arrived.reshape(experts * CAP, -1), precision=lax.Precision.HIGHEST)
    return mixed.astype(jnp.bfloat16)


def solution(mesh):
    in_specs = (
        P("ep", None),
        P(),
        P("ep", None),
        P("ep", None),
        P("ep", None, "tp"),
        P("ep", None, "tp"),
        P("ep", "tp", None),
    )
    out_specs = P("ep", "tp")
    return jax.shard_map(local, mesh=mesh, in_specs=in_specs, out_specs=out_specs, check_vma=False)
```

profile of v0, /device:TPU:0, one launch (start us, length us, event | category | flops | bytes accessed | tf_op | source)
XLA Modules:
  0.0 67.2 jit_solution(11584258141201920099)
XLA Ops:
  6.5 0.0 copy-start
  6.5 0.0 reduce-scatter.2.cloned.1.call-start
  6.5 0.9 %copy.20 = s32[16,2]{1,0:T(8,128)S(1)} copy(s32[16,2]{0,1:T(2,128)} %param.9) | data formatting | bytes 256 | tf_op args[2]
  7.4 0.1 eq.37
  7.5 0.1 fusion.35
  7.6 0.1 reduce_window_sum.11
  7.6 0.2 select_reduce_fusion.1
  7.8 0.9 %fusion.30 = f32[16]{0:T(128)S(1)} fusion(bf16[16,1024]{1,0:T(8,128)(2,1)} %param.7), kind=kLoop, calls=%fused_computation.22 | loop fusion | flops 49136 | bytes 32832 | tf_op jit(solution)/shard_map/reduce_sum | solution.py:20
  8.7 0.8 %fusion.32 = bf16[16,1024]{1,0:T(8,128)(2,1)S(1)} fusion(bf16[16,1024]{1,0:T(8,128)(2,1)} %param.7, f32[1024]{0:T(1024)} %param.8, f32[16]{0:T(128)S(1)} %add_rsqrt_fusion), kind=kLoop, calls=%fused_computation.24 | loop fusion | flops 65536 | bytes 69696 | tf_op jit(solution)/shard_map/convert_element_type | solution.py:21
  9.7 0.2 fusion.18
  9.8 14.5 %all_to_all.10 = bf16[8,8,1024]{2,1,0:T(8,128)(2,1)S(1)} all-to-all(bf16[8,8,1024]{2,1,0:T(8,128)(2,1)S(1)} %fusion.18), channel_id=1, replica_groups=mesh['ep'=8,'tp'=4] {'ep'}, dimensions={0} | all-to-all | bytes 262144 | tf_op jit(solution)/shard_map/all_to_all | solution.py:31
  24.3 1.9 %fusion.6 = f32[8,1,8,896]{3,2,0,1:T(8,128)S(1)} fusion(bf16[8,8,1024]{2,1,0:T(8,128)(2,1)S(1)} %all_to_all.10, bf16[1,1024,896]{2,1,0:T(8,128)(2,1)} %param.11), kind=kOutput, calls=%fused_computation.6 | convolution fusion | flops 117440512 | bytes 2195456 | tf_op jit(solution)/shard_map/secd,edf->secf/dot_general | solution.py:33
  26.2 0.0 copy-done
  26.2 0.0 copy-start.1
  26.2 0.0 copy-start.2
  26.2 2.9 %fusion = f32[8,8,1024]{2,1,0:T(8,128)} fusion(bf16[1,896,1024]{2,1,0:T(8,128)(2,1)S(1)} %copy-done, bf16[8,8,1024]{2,1,0:T(8,128)(2,1)S(1)} %all_to_all.10, bf16[1,1024,896]{2,1,0:T(8,128)(2,1)} %param.12, f32[8,1,8,896]{3,2,0,1:T(8,128)S(1)} %fusion.6), kind=kOutput, calls=%fused_computation | convolution fusion | flops 235225088 | bytes 4292608 | tf_op jit(solution)/shard_map/secf,efd->secd/dot_general | solution.py:36
  29.2 0.0 reduce-scatter.2.cloned.1.call-update
  29.2 0.1 reduce_sum.30
  29.3 0.1 copy.21
  29.4 0.0 copy-done.1
  29.4 17.8 %reduce-scatter.2.cloned.1.call-done = f32[8,8,256]{2,1,0:T(8,128)} async-done(((f32[8,8,1024]{2,1,0:T(8,128)}), f32[8,8,256]{2,1,0:T(8,128)}) %reduce-scatter.2.cloned.1.call-update) | async-done | bytes 65552 | tf_op jit(solution)/shard_map/reduce_scatter | solution.py:40
  47.2 5.5 %all-to-all-start.1 = ((f32[8,8,256]{2,1,0:T(8,128)}), f32[8,8,256]{2,1,0:T(8,128)S(1)}, u32[]{:S(2)}, u32[]{:S(2)}) async-start(f32[8,8,256]{2,1,0:T(8,128)} %reduce-scatter.2.cloned.1.call-done), calls=%async_computation.2 | async-start | bytes 131072 | tf_op jit(solution)/shard_map/all_to_all | solution.py:41
  52.7 0.0 copy-done.2
  52.7 0.1 select_reduce_fusion
  52.8 6.8 %all-to-all-done.1 = f32[8,8,256]{2,1,0:T(8,128)S(1)} async-done(((f32[8,8,256]{2,1,0:T(8,128)}), f32[8,8,256]{2,1,0:T(8,128)S(1)}, u32[]{:S(2)}, u32[]{:S(2)}) %all-to-all-start.1) | async-done | bytes 65568 | tf_op jit(solution)/shard_map/all_to_all | solution.py:41
  59.6 0.7 %convolution_convert_fusion.1 = bf16[16,256]{1,0:T(8,128)(2,1)} fusion(f32[16,64]{1,0:T(8,128)S(1)} %select_reduce_fusion, f32[8,8,256]{2,1,0:T(8,128)S(1)} %all-to-all-done.1), kind=kOutput, calls=%fused_computation.13 | convolution fusion | flops 3149824 | bytes 77824 | tf_op jit(solution)/shard_map/dot_general | solution.py:42
  (5 shorter events, 0.1 us)
Async XLA Ops:
  6.5 19.7 %copy-start = (bf16[1,896,1024]{2,1,0:T(8,128)(2,1)S(1)}, bf16[1,896,1024]{2,1,0:T(8,128)(2,1)}, u32[]{:S(2)}) copy-start(bf16[1,896,1024]{2,1,0:T(8,128)(2,1)} %param.13) | copy-start | bytes 5505028
  6.5 40.6 %reduce-scatter.2.cloned.1.call-start = ((), (), s32[]{:S(2)}) async-start(), calls=%async_computation.3 | async-start | bytes 327680 | tf_op jit(solution)/shard_map/reduce_scatter | solution.py:40
  26.2 3.2 %copy-start.1 = (s32[16,2]{0,1:T(2,128)S(1)}, s32[16,2]{0,1:T(2,128)}, u32[]{:S(2)}) copy-start(s32[16,2]{0,1:T(2,128)} %param.9) | copy-start | bytes 388
  26.2 26.5 %copy-start.2 = (f32[16,2]{0,1:T(2,128)S(1)}, f32[16,2]{0,1:T(2,128)}, u32[]{:S(2)}) copy-start(f32[16,2]{0,1:T(2,128)} %param.10) | copy-start | bytes 388
  47.2 12.4 %all-to-all-start.1 = ((f32[8,8,256]{2,1,0:T(8,128)}), f32[8,8,256]{2,1,0:T(8,128)S(1)}, u32[]{:S(2)}, u32[]{:S(2)}) async-start(f32[8,8,256]{2,1,0:T(8,128)} %reduce-scatter.2.cloned.1.call-done), calls=%async_computation.2 | async-start | bytes 131072 | tf_op jit(solution)/shard_map/all_to_all | solution.py:41
Sparse Core Ops, SparseCore 0:
  29.3 17.8 reduce-scatter.1
where the time goes:
time: 67.6 us; the launch traced here: 67.2 us
  waiting for transfers between devices  24.6 us (36%)
  blocking collectives  14.5 us (21%)
  between operations  13.5 us (20%)
  matrix products  5.76 us (9%)
  starting transfers between devices  5.5 us (8%)
  other arithmetic  2.13 us (3%)
  local copies, waits for them, and re-layouts  1.22 us (2%)
    reduce_scatter x1, waiting for transfers between devices, local(): lax.psum_scatter(partial_out, 'tp', scatter_dimension=2, tiled=True)  17.8 us
    all_to_all x1, blocking collectives, local(): lax.all_to_all(outgoing, 'ep', split_axis=0, concat_axis=0, tiled=True)  14.5 us
    all_to_all x1, waiting for transfers between devices, local(): lax.all_to_all(summed, 'ep', split_axis=0, concat_axis=0, tiled=True)  6.82 us
    all_to_all x1, starting transfers between devices, local(): lax.all_to_all(summed, 'ep', split_axis=0, concat_axis=0, tiled=True)  5.5 us
    dot_general x1, matrix products, local(): jnp.einsum('secf,efd->secd', hidden, w_down, preferred_element_type=jnp.f...  2.94 us
    dot_general x1, matrix products, local(): jnp.einsum('secd,edf->secf', incoming, w_gate, preferred_element_type=jnp...  1.91 us
  transfers between devices with their start and end apart: 2, of which 2 were waited for; matrix products, arithmetic and copies ran while one was open for 0% of the time, Pallas kernels for 0%

commit v1 on v0

v1 whole, which is shorter than its diff:
```python
import functools

import jax
import jax.numpy as jnp
from jax import lax
from jax.experimental import pallas as pl
from jax.experimental.pallas import tpu as pltpu
from jax.sharding import PartitionSpec as P

CAP = 8
MESH = pl.DeviceIdType.MESH

norm_eps = 1e-06


def each(low, high, step):
    if high - low <= 8:
        for index in range(low, high):
            step(index)
    else:
        lax.fori_loop(low, high, lambda index, carry: (step(index), carry)[1], 0)


def kernel(groups, shares, tokens, gain, routing, route_weight, gate_hbm, up_hbm, down_hbm, mixed,
           gate, up, down, outgoing, incoming, partial, arrived, load_sem, send_sem, recv_sem):
    ep, tp = lax.axis_index("ep"), lax.axis_index("tp")
    width = tokens.shape[1]
    part = mixed.shape[1]
    slots = groups * CAP
    cores = 2 if shares % 2 == 0 else 1
    rows = shares // cores

    def toward(q):
        return lax.rem(tp // cores + q // cores, rows) * cores + lax.rem(lax.rem(tp, cores) + q % cores, cores)

    loads = [pltpu.make_async_copy(source.at[0], target, load_sem.at[i])
             for i, (source, target) in enumerate(((gate_hbm, gate), (up_hbm, up), (down_hbm, down)))]
    for load in loads:
        load.start()

    barrier = pltpu.get_barrier_semaphore()
    for q in range(shares):
        peer = toward(q)

        def greet(d):
            pl.semaphore_signal(barrier, inc=1, device_id=(lax.rem(ep + d, groups), peer), device_id_type=MESH)
        each(1 if q == 0 else 0, groups, greet)

    values = tokens[...].astype(jnp.float32)
    scale = lax.rsqrt(jnp.mean(values * values, axis=-1, keepdims=True) + norm_eps)
    normed = (values * scale * gain[...]).astype(jnp.bfloat16)

    count = tokens.shape[0]
    lane = lax.broadcasted_iota(jnp.int32, (count, slots), 1)
    expert = lax.rem(lane // CAP + ep, groups)
    member = jnp.zeros((count, slots), jnp.float32)
    weight = jnp.zeros((count, slots), jnp.float32)
    for k in range(routing.shape[1]):
        named = routing[:, k:k + 1] == expert
        member = jnp.where(named, 1.0, member)
        weight = jnp.where(named, route_weight[:, k:k + 1], weight)
    earlier = lax.broadcasted_iota(jnp.int32, (count, count), 0) > lax.broadcasted_iota(jnp.int32, (count, count), 1)
    before = jnp.dot(jnp.where(earlier, 1.0, 0.0).astype(jnp.bfloat16), member.astype(jnp.bfloat16),
                     preferred_element_type=jnp.float32)
    placed = jnp.where(before == lax.rem(lane, CAP).astype(jnp.float32), member, 0.0)
    weight = weight * placed
    sent = lax.dot_general(placed.astype(jnp.bfloat16), normed, (((0,), (0,)), ((), ())),
                           preferred_element_type=jnp.float32)
    outgoing[...] = sent.reshape(groups, CAP, width).astype(jnp.bfloat16)

    pl.semaphore_wait(barrier, groups * shares - 1)

    def dispatch(d):
        pltpu.make_async_remote_copy(
            src_ref=outgoing.at[d], dst_ref=incoming.at[d], send_sem=send_sem.at[0], recv_sem=recv_sem.at[0],
            device_id=(lax.rem(ep + d, groups), tp), device_id_type=MESH).start()
    each(1, groups, dispatch)
    incoming[0] = outgoing[0]

    loads[0].wait()
    loads[1].wait()
    others = pl.ds(1, groups - 1)
    pltpu.make_async_copy(incoming.at[others], incoming.at[others], recv_sem.at[0]).wait()

    x = incoming[...].astype(jnp.float32).reshape(slots, width).astype(jnp.bfloat16)
    gate_act = jnp.dot(x, gate[...], preferred_element_type=jnp.float32)
    up_act = jnp.dot(x, up[...], preferred_element_type=jnp.float32)
    hidden = (gate_act / (1.0 + jnp.exp(-gate_act)) * up_act).astype(jnp.bfloat16)
    loads[2].wait()

    for q in reversed(range(shares)):
        peer = toward(q)
        columns = pl.ds(pl.multiple_of(peer * part, part), part)
        block = jnp.dot(hidden, down[:, columns], preferred_element_type=jnp.float32)
        partial[q * groups:(q + 1) * groups] = block.reshape(groups, CAP, part)

        def give(d):
            pltpu.make_async_remote_copy(
                src_ref=partial.at[q * groups + d], dst_ref=arrived.at[q * groups + d],
                send_sem=send_sem.at[1], recv_sem=recv_sem.at[1],
                device_id=(lax.rem(ep - d + groups, groups), peer), device_id_type=MESH).start()
        each(1 if q == 0 else 0, groups, give)
    arrived[0] = partial[0]

    rest = pl.ds(1, groups * shares - 1)
    pltpu.make_async_copy(arrived.at[rest], arrived.at[rest], recv_sem.at[1]).wait()
    total = arrived[0:groups]
    for q in range(1, shares):
        total = total + arrived[q * groups:(q + 1) * groups]
    out = jnp.dot(weight, total.reshape(slots, part), precision=lax.Precision.HIGHEST,
                  preferred_element_type=jnp.float32)
    mixed[...] = out.astype(mixed.dtype)
    pltpu.make_async_copy(outgoing.at[others], outgoing.at[others], send_sem.at[0]).wait()
    pltpu.make_async_copy(partial.at[rest], partial.at[rest], send_sem.at[1]).wait()


def solution(mesh):
    groups, shares = mesh.shape["ep"], mesh.shape["tp"]

    def local(tokens, norm_gain, routing, route_weight, w_gate, w_up, w_down):
        count, width = tokens.shape
        part = width // shares
        vmem = pl.BlockSpec(memory_space=pltpu.VMEM)
        hbm = pl.BlockSpec(memory_space=pltpu.HBM)
        return pl.pallas_call(
            functools.partial(kernel, groups, shares),
            out_shape=jax.ShapeDtypeStruct((count, part), jnp.bfloat16),
            in_specs=[vmem] * 4 + [hbm] * 3,
            out_specs=vmem,
            scratch_shapes=[
                pltpu.VMEM(w_gate.shape[1:], jnp.bfloat16),
                pltpu.VMEM(w_up.shape[1:], jnp.bfloat16),
                pltpu.VMEM(w_down.shape[1:], jnp.bfloat16),
                pltpu.VMEM((groups, CAP, width), jnp.bfloat16),
                pltpu.VMEM((groups, CAP, width), jnp.bfloat16),
                pltpu.VMEM((groups * shares, CAP, part), jnp.float32),
                pltpu.VMEM((groups * shares, CAP, part), jnp.float32),
                pltpu.SemaphoreType.DMA((3,)),
                pltpu.SemaphoreType.DMA((2,)),
                pltpu.SemaphoreType.DMA((2,)),
            ],
            compiler_params=pltpu.CompilerParams(collective_id=0, has_side_effects=True,
                                                 vmem_limit_bytes=40 * 1024 * 1024),
            name="experts",
        )(tokens, norm_gain.reshape(1, width), routing, route_weight, w_gate, w_up, w_down)

    in_specs = (
        P("ep", None),
        P(),
        P("ep", None),
        P("ep", None),
        P("ep", None, "tp"),
        P("ep", None, "tp"),
        P("ep", "tp", None),
    )
    return jax.shard_map(local, mesh=mesh, in_specs=in_specs, out_specs=P("ep", "tp"), check_vma=False)
```

time: 67.6 us -> 29.5 us (0.44)
  waiting for transfers between devices: 24.6 us -> 0 us
  Pallas kernels: 0 us -> 21.1 us
  blocking collectives: 14.5 us -> 0 us
  between operations: 13.5 us -> 0.02 us
  local copies, waits for them, and re-layouts: 1.22 us -> 8.05 us
  matrix products: 5.76 us -> 0 us
  starting transfers between devices: 5.5 us -> 0 us
  other arithmetic: 2.13 us -> 0 us
    pallas_call x0 -> x1, Pallas kernels: none -> 21.1 us  [local(): pl.pallas_call(functools.partial(kernel, groups, shares), out_shape=jax.S...]
    reduce_scatter x1 -> x0, waiting for transfers between devices: 17.8 us -> none  [local(): lax.psum_scatter(partial_out, 'tp', scatter_dimension=2, tiled=True)]
    all_to_all x1 -> x0, blocking collectives: 14.5 us -> none  [local(): lax.all_to_all(outgoing, 'ep', split_axis=0, concat_axis=0, tiled=True)]
    unnamed x7 -> x13, local copies, waits for them, and re-layouts: 0.91 us -> 8.05 us
    all_to_all x1 -> x0, waiting for transfers between devices: 6.82 us -> none  [local(): lax.all_to_all(summed, 'ep', split_axis=0, concat_axis=0, tiled=True)]
    dot_general x4 -> x0, matrix products: 5.76 us -> none  [the longest x1 2.94 us: local(): jnp.einsum('secf,efd->secd', hidden, w_down, preferred_element_type=jnp.f...]
    all_to_all x1 -> x0, starting transfers between devices: 5.5 us -> none  [local(): lax.all_to_all(summed, 'ep', split_axis=0, concat_axis=0, tiled=True)]
    reduce_sum x3 -> x0, other arithmetic: 1.14 us -> none  [the longest x1 0.88 us: local(): jnp.mean(values * values, axis=-1, keepdims=True) + norm_eps]
  transfers between devices with their start and end apart: 2 -> 0, of which waited for: 2 -> 0; matrix products, arithmetic and copies ran while one was open for 0% -> 0% of each run, Pallas kernels for 0% -> 0%
where the time goes in v1:
time: 29.5 us; the launch traced here: 29.2 us
  Pallas kernels  21.1 us (72%)
  local copies, waits for them, and re-layouts  8.05 us (27%)
    pallas_call x1, Pallas kernels, local(): pl.pallas_call(functools.partial(kernel, groups, shares), out_shape=jax.S...  21.1 us
    unnamed x13, local copies, waits for them, and re-layouts  8.05 us

profile of v1, /device:TPU:0, one launch (start us, length us, event | category | flops | bytes accessed | tf_op | source)
XLA Modules:
  0.0 29.2 jit_solution(13201336133094951150)
XLA Ops:
  0.0 0.8 %copy.8.routing = s32[16,2]{1,0:T(8,128)S(1)} copy(s32[16,2]{0,1:T(2,128)} %param.9) | data formatting | bytes 256 | tf_op args[2]
  0.8 0.8 %copy.9.route_weight = f32[16,2]{1,0:T(8,128)S(1)} copy(f32[16,2]{0,1:T(2,128)} %param.10) | data formatting | bytes 256 | tf_op args[3]
  1.5 0.0 copy-start
  1.5 1.5 %copy-done = bf16[1,1024,896]{2,1,0:T(8,128)(2,1)S(1)} copy-done((bf16[1,1024,896]{2,1,0:T(8,128)(2,1)S(1)}, bf16[1,1024,896]{2,1,0:T(8,128)(2,1)}, u32[]{:S(2)}) %copy-start) | copy-done | bytes 1835032
  3.0 0.0 copy-start.1
  3.0 1.5 %copy-done.1 = bf16[1,1024,896]{2,1,0:T(8,128)(2,1)S(1)} copy-done((bf16[1,1024,896]{2,1,0:T(8,128)(2,1)S(1)}, bf16[1,1024,896]{2,1,0:T(8,128)(2,1)}, u32[]{:S(2)}) %copy-start.1) | copy-done | bytes 1835032
  4.5 0.0 copy-start.2
  4.5 1.5 %copy-done.2 = bf16[1,896,1024]{2,1,0:T(8,128)(2,1)S(1)} copy-done((bf16[1,896,1024]{2,1,0:T(8,128)(2,1)S(1)}, bf16[1,896,1024]{2,1,0:T(8,128)(2,1)}, u32[]{:S(2)}) %copy-start.2) | copy-done | bytes 1835032
  6.0 0.0 copy-start.3
  6.0 0.8 %copy-done.3 = bf16[16,1024]{1,0:T(8,128)(2,1)S(1)} copy-done((bf16[16,1024]{1,0:T(8,128)(2,1)S(1)}, bf16[16,1024]{1,0:T(8,128)(2,1)}, u32[]{:S(2)}) %copy-start.3) | copy-done | bytes 32792
  6.8 0.0 copy-start.4
  6.8 0.7 %copy-done.4 = f32[1024]{0:T(1024)S(1)} copy-done((f32[1024]{0:T(1024)S(1)}, f32[1024]{0:T(1024)}, u32[]{:S(2)}) %copy-start.4) | copy-done | bytes 4120
  7.5 21.1 %experts.1 = bf16[16,256]{1,0:T(8,128)(2,1)S(1)} custom-call(bf16[16,1024]{1,0:T(8,128)(2,1)S(1)} %copy-done.3, f32[1,1024]{1,0:T(1,128)S(1)} %bitcast.1, s32[16,2]{1,0:T(8,128)S(1)} %copy.8.routing, f32[16,2]{1,0:T(8,128)S(1)} %copy.9.route_weight, bf16[1,1024,896]{2,1,0:T(8,128)(2,1)S(1)} %copy-done, bf16[1,1024,896]{2,1,0:T(8,128)(2,1)S(1)} %copy-done.1, ...), custom_call_target="tpu_custom_call" | custom-call | tf_op jit(solution)/shard_map/experts/pallas_call | solution.py:125
  28.6 0.6 %copy.11 = bf16[16,256]{1,0:T(8,128)(2,1)} copy(bf16[16,256]{1,0:T(8,128)(2,1)S(1)} %experts.1) | data formatting | bytes 16384
Async XLA Ops:
  1.5 1.5 %copy-start = (bf16[1,1024,896]{2,1,0:T(8,128)(2,1)S(1)}, bf16[1,1024,896]{2,1,0:T(8,128)(2,1)}, u32[]{:S(2)}) copy-start(bf16[1,1024,896]{2,1,0:T(8,128)(2,1)} %gate_hbm.1) | copy-start | bytes 5505028
  3.0 1.5 %copy-start.1 = (bf16[1,1024,896]{2,1,0:T(8,128)(2,1)S(1)}, bf16[1,1024,896]{2,1,0:T(8,128)(2,1)}, u32[]{:S(2)}) copy-start(bf16[1,1024,896]{2,1,0:T(8,128)(2,1)} %up_hbm.1) | copy-start | bytes 5505028
  4.5 1.5 %copy-start.2 = (bf16[1,896,1024]{2,1,0:T(8,128)(2,1)S(1)}, bf16[1,896,1024]{2,1,0:T(8,128)(2,1)}, u32[]{:S(2)}) copy-start(bf16[1,896,1024]{2,1,0:T(8,128)(2,1)} %down_hbm.1) | copy-start | bytes 5505028
  6.0 0.8 %copy-start.3 = (bf16[16,1024]{1,0:T(8,128)(2,1)S(1)}, bf16[16,1024]{1,0:T(8,128)(2,1)}, u32[]{:S(2)}) copy-start(bf16[16,1024]{1,0:T(8,128)(2,1)} %tokens.1) | copy-start | bytes 98308
  6.8 0.7 %copy-start.4 = (f32[1024]{0:T(1024)S(1)}, f32[1024]{0:T(1024)}, u32[]{:S(2)}) copy-start(f32[1024]{0:T(1024)} %param.8) | copy-start | bytes 12292

commit v2 on v1

--- a/solution.py
+++ b/solution.py
@@ -21,7 +21,8 @@
         lax.fori_loop(low, high, lambda index, carry: (step(index), carry)[1], 0)
 
 
-def kernel(groups, shares, tokens, gain, routing, route_weight, gate_hbm, up_hbm, down_hbm, mixed,
+def kernel(groups, shares, tokens_hbm, gain_hbm, routing_hbm, route_weight_hbm, gate_hbm, up_hbm, down_hbm, mixed,
+           tokens, gain, routing, route_weight,
            gate, up, down, outgoing, incoming, partial, arrived, load_sem, send_sem, recv_sem):
     ep, tp = lax.axis_index("ep"), lax.axis_index("tp")
     width = tokens.shape[1]
@@ -33,42 +34,46 @@
     def toward(q):
         return lax.rem(tp // cores + q // cores, rows) * cores + lax.rem(lax.rem(tp, cores) + q % cores, cores)
 
-    loads = [pltpu.make_async_copy(source.at[0], target, load_sem.at[i])
-             for i, (source, target) in enumerate(((gate_hbm, gate), (up_hbm, up), (down_hbm, down)))]
+    pairs = ((tokens_hbm, tokens), (gain_hbm, gain), (routing_hbm, routing), (route_weight_hbm, route_weight),
+             (gate_hbm.at[0], gate), (up_hbm.at[0], up), (down_hbm.at[0], down))
+    loads = [pltpu.make_async_copy(source, target, load_sem.at[i]) for i, (source, target) in enumerate(pairs)]
     for load in loads:
         load.start()
 
     barrier = pltpu.get_barrier_semaphore()
-    for q in range(shares):
-        peer = toward(q)
 
-        def greet(d):
-            pl.semaphore_signal(barrier, inc=1, device_id=(lax.rem(ep + d, groups), peer), device_id_type=MESH)
-        each(1 if q == 0 else 0, groups, greet)
+    def greet(d):
+        pl.semaphore_signal(barrier, inc=1, device_id=(lax.rem(ep + d, groups), tp), device_id_type=MESH)
+    each(1, groups, greet)
+    for q in range(1, shares):
+        pl.semaphore_signal(barrier, inc=1, device_id=(ep, toward(q)), device_id_type=MESH)
 
+    count = tokens.shape[0]
+    line = lax.broadcasted_iota(jnp.int32, (slots, count), 0)
+    expert = lax.rem(line // CAP + ep, groups)
+    member = jnp.zeros((slots, count), jnp.float32)
+    weight = jnp.zeros((slots, count), jnp.float32)
+    loads[2].wait()
+    loads[3].wait()
+    for k in range(routing.shape[0]):
+        named = routing[k:k + 1, :] == expert
+        member = jnp.where(named, 1.0, member)
+        weight = jnp.where(named, route_weight[k:k + 1, :], weight)
+    earlier = lax.broadcasted_iota(jnp.int32, (count, count), 0) < lax.broadcasted_iota(jnp.int32, (count, count), 1)
+    before = jnp.dot(member.astype(jnp.bfloat16), jnp.where(earlier, 1.0, 0.0).astype(jnp.bfloat16),
+                     preferred_element_type=jnp.float32)
+    placed = jnp.where(before == lax.rem(line, CAP).astype(jnp.float32), member, 0.0)
+    weight = jnp.transpose(weight * placed)
+
+    loads[0].wait()
+    loads[1].wait()
     values = tokens[...].astype(jnp.float32)
     scale = lax.rsqrt(jnp.mean(values * values, axis=-1, keepdims=True) + norm_eps)
     normed = (values * scale * gain[...]).astype(jnp.bfloat16)
-
-    count = tokens.shape[0]
-    lane = lax.broadcasted_iota(jnp.int32, (count, slots), 1)
-    expert = lax.rem(lane // CAP + ep, groups)
-    member = jnp.zeros((count, slots), jnp.float32)
-    weight = jnp.zeros((count, slots), jnp.float32)
-    for k in range(routing.shape[1]):
-        named = routing[:, k:k + 1] == expert
-        member = jnp.where(named, 1.0, member)
-        weight = jnp.where(named, route_weight[:, k:k + 1], weight)
-    earlier = lax.broadcasted_iota(jnp.int32, (count, count), 0) > lax.broadcasted_iota(jnp.int32, (count, count), 1)
-    before = jnp.dot(jnp.where(earlier, 1.0, 0.0).astype(jnp.bfloat16), member.astype(jnp.bfloat16),
-                     preferred_element_type=jnp.float32)
-    placed = jnp.where(before == lax.rem(lane, CAP).astype(jnp.float32), member, 0.0)
-    weight = weight * placed
-    sent = lax.dot_general(placed.astype(jnp.bfloat16), normed, (((0,), (0,)), ((), ())),
-                           preferred_element_type=jnp.float32)
+    sent = jnp.dot(placed.astype(jnp.bfloat16), normed, preferred_element_type=jnp.float32)
     outgoing[...] = sent.reshape(groups, CAP, width).astype(jnp.bfloat16)
 
-    pl.semaphore_wait(barrier, groups * shares - 1)
+    pl.semaphore_wait(barrier, groups + shares - 2)
 
     def dispatch(d):
         pltpu.make_async_remote_copy(
@@ -77,8 +82,8 @@
     each(1, groups, dispatch)
     incoming[0] = outgoing[0]
 
-    loads[0].wait()
-    loads[1].wait()
+    loads[4].wait()
+    loads[5].wait()
     others = pl.ds(1, groups - 1)
     pltpu.make_async_copy(incoming.at[others], incoming.at[others], recv_sem.at[0]).wait()
 
@@ -86,7 +91,7 @@
     gate_act = jnp.dot(x, gate[...], preferred_element_type=jnp.float32)
     up_act = jnp.dot(x, up[...], preferred_element_type=jnp.float32)
     hidden = (gate_act / (1.0 + jnp.exp(-gate_act)) * up_act).astype(jnp.bfloat16)
-    loads[2].wait()
+    loads[6].wait()
 
     for q in reversed(range(shares)):
         peer = toward(q)
@@ -125,9 +130,13 @@
         return pl.pallas_call(
             functools.partial(kernel, groups, shares),
             out_shape=jax.ShapeDtypeStruct((count, part), jnp.bfloat16),
-            in_specs=[vmem] * 4 + [hbm] * 3,
+            in_specs=[hbm] * 7,
             out_specs=vmem,
             scratch_shapes=[
+                pltpu.VMEM((count, width), tokens.dtype),
+                pltpu.VMEM((1, width), norm_gain.dtype),
+                pltpu.VMEM(routing.shape[::-1], routing.dtype),
+                pltpu.VMEM(route_weight.shape[::-1], route_weight.dtype),
                 pltpu.VMEM(w_gate.shape[1:], jnp.bfloat16),
                 pltpu.VMEM(w_up.shape[1:], jnp.bfloat16),
                 pltpu.VMEM(w_down.shape[1:], jnp.bfloat16),
@@ -135,14 +144,14 @@
                 pltpu.VMEM((groups, CAP, width), jnp.bfloat16),
                 pltpu.VMEM((groups * shares, CAP, part), jnp.float32),
                 pltpu.VMEM((groups * shares, CAP, part), jnp.float32),
-                pltpu.SemaphoreType.DMA((3,)),
+                pltpu.SemaphoreType.DMA((7,)),
                 pltpu.SemaphoreType.DMA((2,)),
                 pltpu.SemaphoreType.DMA((2,)),
             ],
             compiler_params=pltpu.CompilerParams(collective_id=0, has_side_effects=True,
-                                                 vmem_limit_bytes=40 * 1024 * 1024),
+                                                 vmem_limit_bytes=67043328),
             name="experts",
-        )(tokens, norm_gain.reshape(1, width), routing, route_weight, w_gate, w_up, w_down)
+        )(tokens, norm_gain.reshape(1, width), routing.T, route_weight.T, w_gate, w_up, w_down)
 
     in_specs = (
         P("ep", None),

time: 29.5 us -> 20.9 us (0.71)
  local copies, waits for them, and re-layouts: 8.05 us -> 1.3 us
  Pallas kernels: 21.1 us -> 19.4 us
    unnamed x13 -> x1, local copies, waits for them, and re-layouts: 8.05 us -> 1.3 us
    pallas_call x1, Pallas kernels: 21.1 us -> 19.4 us  [local(): pl.pallas_call(functools.partial(kernel, groups, shares), out_shape=jax.S...]
where the time goes in v2:
time: 20.9 us; the launch traced here: 20.7 us
  Pallas kernels  19.4 us (93%)
  local copies, waits for them, and re-layouts  1.3 us (6%)
    pallas_call x1, Pallas kernels, local(): pl.pallas_call(functools.partial(kernel, groups, shares), out_shape=jax.S...  19.4 us
    unnamed x1, local copies, waits for them, and re-layouts  1.3 us

profile of v2, /device:TPU:0, one launch (start us, length us, event | category | flops | bytes accessed | tf_op | source)
XLA Modules:
  0.0 20.7 jit_solution(6309543901228639610)
XLA Ops:
  0.0 19.4 %experts.1 = bf16[16,256]{1,0:T(8,128)(2,1)} custom-call(bf16[16,1024]{1,0:T(8,128)(2,1)} %tokens_hbm.1, f32[1,1024]{1,0:T(1,128)} %bitcast.3, s32[2,16]{1,0:T(2,128)} %bitcast.4, f32[2,16]{1,0:T(2,128)} %bitcast.5, bf16[1,1024,896]{2,1,0:T(8,128)(2,1)} %gate_hbm.1, bf16[1,1024,896]{2,1,0:T(8,128)(2,1)} %up_hbm.1, bf16[1,896,1024]{2,1,0:T(8,128)(2,1)} %down_hbm.1), custom_call_target="tpu_custom_call" | custom-call | tf_op jit(solution)/shard_map/experts/pallas_call | solution.py:130
  19.4 1.3 %copy.9 = bf16[16,256]{1,0:T(8,128)(2,1)} copy(bf16[16,256]{1,0:T(8,128)(2,1)} %experts.1) | data formatting | bytes 16384

commit v3 on v2

--- a/solution.py
+++ b/solution.py
@@ -23,16 +23,16 @@
 
 def kernel(groups, shares, tokens_hbm, gain_hbm, routing_hbm, route_weight_hbm, gate_hbm, up_hbm, down_hbm, mixed,
            tokens, gain, routing, route_weight,
-           gate, up, down, outgoing, incoming, partial, arrived, load_sem, send_sem, recv_sem):
+           gate, up, down, outgoing, incoming, lent, borrowed, partial, arrived, load_sem, send_sem, recv_sem):
     ep, tp = lax.axis_index("ep"), lax.axis_index("tp")
     width = tokens.shape[1]
     part = mixed.shape[1]
     slots = groups * CAP
-    cores = 2 if shares % 2 == 0 else 1
-    rows = shares // cores
+    rows = shares // 2
+    row, core = tp // 2, lax.rem(tp, 2)
 
     def toward(q):
-        return lax.rem(tp // cores + q // cores, rows) * cores + lax.rem(lax.rem(tp, cores) + q % cores, cores)
+        return lax.rem(row + q // 2, rows) * 2 + lax.rem(core + q % 2, 2)
 
     pairs = ((tokens_hbm, tokens), (gain_hbm, gain), (routing_hbm, routing), (route_weight_hbm, route_weight),
              (gate_hbm.at[0], gate), (up_hbm.at[0], up), (down_hbm.at[0], down))
@@ -45,7 +45,7 @@
     def greet(d):
         pl.semaphore_signal(barrier, inc=1, device_id=(lax.rem(ep + d, groups), tp), device_id_type=MESH)
     each(1, groups, greet)
-    for q in range(1, shares):
+    for q in [1] + [2 * q for q in range(1, rows)]:
         pl.semaphore_signal(barrier, inc=1, device_id=(ep, toward(q)), device_id_type=MESH)
 
     count = tokens.shape[0]
@@ -73,7 +73,7 @@
     sent = jnp.dot(placed.astype(jnp.bfloat16), normed, preferred_element_type=jnp.float32)
     outgoing[...] = sent.reshape(groups, CAP, width).astype(jnp.bfloat16)
 
-    pl.semaphore_wait(barrier, groups + shares - 2)
+    pl.semaphore_wait(barrier, groups + rows - 1)
 
     def dispatch(d):
         pltpu.make_async_remote_copy(
@@ -93,30 +93,43 @@
     hidden = (gate_act / (1.0 + jnp.exp(-gate_act)) * up_act).astype(jnp.bfloat16)
     loads[6].wait()
 
-    for q in reversed(range(shares)):
-        peer = toward(q)
-        columns = pl.ds(pl.multiple_of(peer * part, part), part)
-        block = jnp.dot(hidden, down[:, columns], preferred_element_type=jnp.float32)
-        partial[q * groups:(q + 1) * groups] = block.reshape(groups, CAP, part)
+    def block_of(q, side):
+        columns = pl.ds(pl.multiple_of((lax.rem(row + q, rows) * 2 + side) * part, part), part)
+        return jnp.dot(hidden, down[:, columns], preferred_element_type=jnp.float32)
+
+    lends = []
+    for q in reversed(range(rows)):
+        lent[q] = block_of(q, 1 - core)
+        lends.append(pltpu.make_async_remote_copy(
+            src_ref=lent.at[q], dst_ref=borrowed.at[q], send_sem=send_sem.at[2 + q], recv_sem=recv_sem.at[2 + q],
+            device_id=(ep, row * 2 + 1 - core), device_id_type=MESH))
+        lends[-1].start()
+
+    for q, lend in zip(reversed(range(rows)), lends):
+        block = block_of(q, core)
+        lend.wait_recv()
+        partial[q * groups:(q + 1) * groups] = (block + borrowed[q]).reshape(groups, CAP, part)
 
         def give(d):
             pltpu.make_async_remote_copy(
                 src_ref=partial.at[q * groups + d], dst_ref=arrived.at[q * groups + d],
                 send_sem=send_sem.at[1], recv_sem=recv_sem.at[1],
-                device_id=(lax.rem(ep - d + groups, groups), peer), device_id_type=MESH).start()
+                device_id=(lax.rem(ep - d + groups, groups), toward(2 * q)), device_id_type=MESH).start()
         each(1 if q == 0 else 0, groups, give)
     arrived[0] = partial[0]
 
-    rest = pl.ds(1, groups * shares - 1)
+    rest = pl.ds(1, groups * rows - 1)
     pltpu.make_async_copy(arrived.at[rest], arrived.at[rest], recv_sem.at[1]).wait()
     total = arrived[0:groups]
-    for q in range(1, shares):
+    for q in range(1, rows):
         total = total + arrived[q * groups:(q + 1) * groups]
     out = jnp.dot(weight, total.reshape(slots, part), precision=lax.Precision.HIGHEST,
                   preferred_element_type=jnp.float32)
     mixed[...] = out.astype(mixed.dtype)
     pltpu.make_async_copy(outgoing.at[others], outgoing.at[others], send_sem.at[0]).wait()
     pltpu.make_async_copy(partial.at[rest], partial.at[rest], send_sem.at[1]).wait()
+    for lend in lends:
+        lend.wait_send()
 
 
 def solution(mesh):
@@ -142,14 +155,16 @@
                 pltpu.VMEM(w_down.shape[1:], jnp.bfloat16),
                 pltpu.VMEM((groups, CAP, width), jnp.bfloat16),
                 pltpu.VMEM((groups, CAP, width), jnp.bfloat16),
-                pltpu.VMEM((groups * shares, CAP, part), jnp.float32),
-                pltpu.VMEM((groups * shares, CAP, part), jnp.float32),
+                pltpu.VMEM((shares // 2, groups * CAP, part), jnp.float32),
+                pltpu.VMEM((shares // 2, groups * CAP, part), jnp.float32),
+                pltpu.VMEM((groups * shares // 2, CAP, part), jnp.float32),
+                pltpu.VMEM((groups * shares // 2, CAP, part), jnp.float32),
                 pltpu.SemaphoreType.DMA((7,)),
-                pltpu.SemaphoreType.DMA((2,)),
-                pltpu.SemaphoreType.DMA((2,)),
+                pltpu.SemaphoreType.DMA((2 + shares // 2,)),
+                pltpu.SemaphoreType.DMA((2 + shares // 2,)),
             ],
             compiler_params=pltpu.CompilerParams(collective_id=0, has_side_effects=True,
-                                                 vmem_limit_bytes=67043328),
+                                                 vmem_limit_bytes=67043328 - 16384),
             name="experts",
         )(tokens, norm_gain.reshape(1, width), routing.T, route_weight.T, w_gate, w_up, w_down)
 

time: 20.9 us -> 21.3 us (1.019)
  Pallas kernels: 19.4 us -> 19.7 us
    pallas_call x1, Pallas kernels: 19.4 us -> 19.7 us  [local(): pl.pallas_call(functools.partial(kernel, groups, shares), out_shape=jax.S...]
where the time goes in v3:
time: 21.3 us; the launch traced here: 21.1 us
  Pallas kernels  19.7 us (92%)
  local copies, waits for them, and re-layouts  1.3 us (6%)
    pallas_call x1, Pallas kernels, local(): pl.pallas_call(functools.partial(kernel, groups, shares), out_shape=jax.S...  19.7 us
    unnamed x1, local copies, waits for them, and re-layouts  1.3 us

profile of v3, /device:TPU:0, one launch (start us, length us, event | category | flops | bytes accessed | tf_op | source)
XLA Modules:
  0.0 21.1 jit_solution(9020662801711622112)
XLA Ops:
  0.0 19.7 %experts.1 = bf16[16,256]{1,0:T(8,128)(2,1)} custom-call(bf16[16,1024]{1,0:T(8,128)(2,1)} %tokens_hbm.1, f32[1,1024]{1,0:T(1,128)} %bitcast.3, s32[2,16]{1,0:T(2,128)} %bitcast.4, f32[2,16]{1,0:T(2,128)} %bitcast.5, bf16[1,1024,896]{2,1,0:T(8,128)(2,1)} %gate_hbm.1, bf16[1,1024,896]{2,1,0:T(8,128)(2,1)} %up_hbm.1, bf16[1,896,1024]{2,1,0:T(8,128)(2,1)} %down_hbm.1), custom_call_target="tpu_custom_call" | custom-call | tf_op jit(solution)/shard_map/experts/pallas_call | solution.py:143
  19.8 1.3 %copy.9 = bf16[16,256]{1,0:T(8,128)(2,1)} copy(bf16[16,256]{1,0:T(8,128)(2,1)} %experts.1) | data formatting | bytes 16384

commit v4 on v2

--- a/solution.py
+++ b/solution.py
@@ -23,16 +23,19 @@
 
 def kernel(groups, shares, tokens_hbm, gain_hbm, routing_hbm, route_weight_hbm, gate_hbm, up_hbm, down_hbm, mixed,
            tokens, gain, routing, route_weight,
-           gate, up, down, outgoing, incoming, partial, arrived, load_sem, send_sem, recv_sem):
+           gate, up, down, outgoing, incoming, lent, borrowed, partial, arrived, load_sem, send_sem, recv_sem):
     ep, tp = lax.axis_index("ep"), lax.axis_index("tp")
     width = tokens.shape[1]
     part = mixed.shape[1]
     slots = groups * CAP
-    cores = 2 if shares % 2 == 0 else 1
-    rows = shares // cores
+    rows = shares // 2
+    row, core = tp // 2, lax.rem(tp, 2)
 
     def toward(q):
-        return lax.rem(tp // cores + q // cores, rows) * cores + lax.rem(lax.rem(tp, cores) + q % cores, cores)
+        return lax.rem(row + q // 2, rows) * 2 + lax.rem(core + q % 2, 2)
+
+    def far_first(step):
+        return step + (1 - 2 * ep // groups) * (groups - 1 - 2 * step)
 
     pairs = ((tokens_hbm, tokens), (gain_hbm, gain), (routing_hbm, routing), (route_weight_hbm, route_weight),
              (gate_hbm.at[0], gate), (up_hbm.at[0], up), (down_hbm.at[0], down))
@@ -93,30 +96,53 @@
     hidden = (gate_act / (1.0 + jnp.exp(-gate_act)) * up_act).astype(jnp.bfloat16)
     loads[6].wait()
 
-    for q in reversed(range(shares)):
-        peer = toward(q)
-        columns = pl.ds(pl.multiple_of(peer * part, part), part)
-        block = jnp.dot(hidden, down[:, columns], preferred_element_type=jnp.float32)
-        partial[q * groups:(q + 1) * groups] = block.reshape(groups, CAP, part)
+    def block_of(q, side):
+        columns = pl.ds(pl.multiple_of((lax.rem(row + q, rows) * 2 + side) * part, part), part)
+        return jnp.dot(hidden, down[:, columns], preferred_element_type=jnp.float32)
 
-        def give(d):
-            pltpu.make_async_remote_copy(
-                src_ref=partial.at[q * groups + d], dst_ref=arrived.at[q * groups + d],
-                send_sem=send_sem.at[1], recv_sem=recv_sem.at[1],
-                device_id=(lax.rem(ep - d + groups, groups), peer), device_id_type=MESH).start()
-        each(1 if q == 0 else 0, groups, give)
+    def give(place, q):
+        def to(step):
+            target = far_first(step)
+
+            def copy():
+                d = lax.rem(ep - target + groups, groups)
+                pltpu.make_async_remote_copy(
+                    src_ref=partial.at[place * groups + d], dst_ref=arrived.at[place * groups + d],
+                    send_sem=send_sem.at[1], recv_sem=recv_sem.at[1],
+                    device_id=(target, toward(q)), device_id_type=MESH).start()
+            if q == 0:
+                pl.when(target != ep)(copy)
+            else:
+                copy()
+        each(0, groups, to)
+
+    for q in range(2, shares):
+        block = block_of(q // 2, lax.rem(core + q, 2))
+        partial[(q - 1) * groups:q * groups] = block.reshape(groups, CAP, part)
+        give(q - 1, q)
+
+    lent[...] = block_of(0, 1 - core)
+    lend = pltpu.make_async_remote_copy(
+        src_ref=lent, dst_ref=borrowed, send_sem=send_sem.at[2], recv_sem=recv_sem.at[2],
+        device_id=(ep, toward(1)), device_id_type=MESH)
+    lend.start()
+    block = block_of(0, core)
+    lend.wait_recv()
+    partial[0:groups] = (block + borrowed[...]).reshape(groups, CAP, part)
+    give(0, 0)
     arrived[0] = partial[0]
 
-    rest = pl.ds(1, groups * shares - 1)
+    rest = pl.ds(1, groups * (shares - 1) - 1)
     pltpu.make_async_copy(arrived.at[rest], arrived.at[rest], recv_sem.at[1]).wait()
     total = arrived[0:groups]
-    for q in range(1, shares):
+    for q in range(1, shares - 1):
         total = total + arrived[q * groups:(q + 1) * groups]
     out = jnp.dot(weight, total.reshape(slots, part), precision=lax.Precision.HIGHEST,
                   preferred_element_type=jnp.float32)
     mixed[...] = out.astype(mixed.dtype)
     pltpu.make_async_copy(outgoing.at[others], outgoing.at[others], send_sem.at[0]).wait()
     pltpu.make_async_copy(partial.at[rest], partial.at[rest], send_sem.at[1]).wait()
+    lend.wait_send()
 
 
 def solution(mesh):
@@ -142,11 +168,13 @@
                 pltpu.VMEM(w_down.shape[1:], jnp.bfloat16),
                 pltpu.VMEM((groups, CAP, width), jnp.bfloat16),
                 pltpu.VMEM((groups, CAP, width), jnp.bfloat16),
-                pltpu.VMEM((groups * shares, CAP, part), jnp.float32),
-                pltpu.VMEM((groups * shares, CAP, part), jnp.float32),
+                pltpu.VMEM((groups * CAP, part), jnp.float32),
+                pltpu.VMEM((groups * CAP, part), jnp.float32),
+                pltpu.VMEM((groups * (shares - 1), CAP, part), jnp.float32),
+                pltpu.VMEM((groups * (shares - 1), CAP, part), jnp.float32),
                 pltpu.SemaphoreType.DMA((7,)),
-                pltpu.SemaphoreType.DMA((2,)),
-                pltpu.SemaphoreType.DMA((2,)),
+                pltpu.SemaphoreType.DMA((3,)),
+                pltpu.SemaphoreType.DMA((3,)),
             ],
             compiler_params=pltpu.CompilerParams(collective_id=0, has_side_effects=True,
                                                  vmem_limit_bytes=67043328),

time: 20.9 us -> 19.9 us (0.952)
  Pallas kernels: 19.4 us -> 18.4 us
    pallas_call x1, Pallas kernels: 19.4 us -> 18.4 us  [local(): pl.pallas_call(functools.partial(kernel, groups, shares), out_shape=jax.S...]
where the time goes in v4:
time: 19.9 us; the launch traced here: 19.7 us
  Pallas kernels  18.4 us (92%)
  local copies, waits for them, and re-layouts  1.3 us (7%)
    pallas_call x1, Pallas kernels, local(): pl.pallas_call(functools.partial(kernel, groups, shares), out_shape=jax.S...  18.4 us
    unnamed x1, local copies, waits for them, and re-layouts  1.3 us

profile of v4, /device:TPU:0, one launch (start us, length us, event | category | flops | bytes accessed | tf_op | source)
XLA Modules:
  0.0 19.7 jit_solution(3914439356654316174)
XLA Ops:
  0.0 18.4 %experts.1 = bf16[16,256]{1,0:T(8,128)(2,1)} custom-call(bf16[16,1024]{1,0:T(8,128)(2,1)} %tokens_hbm.1, f32[1,1024]{1,0:T(1,128)} %bitcast.3, s32[2,16]{1,0:T(2,128)} %bitcast.4, f32[2,16]{1,0:T(2,128)} %bitcast.5, bf16[1,1024,896]{2,1,0:T(8,128)(2,1)} %gate_hbm.1, bf16[1,1024,896]{2,1,0:T(8,128)(2,1)} %up_hbm.1, bf16[1,896,1024]{2,1,0:T(8,128)(2,1)} %down_hbm.1), custom_call_target="tpu_custom_call" | custom-call | tf_op jit(solution)/shard_map/experts/pallas_call | solution.py:156
  18.4 1.3 %copy.9 = bf16[16,256]{1,0:T(8,128)(2,1)} copy(bf16[16,256]{1,0:T(8,128)(2,1)} %experts.1) | data formatting | bytes 16384

commit v5 on v4

--- a/solution.py
+++ b/solution.py
@@ -87,6 +87,7 @@
 
     loads[4].wait()
     loads[5].wait()
+    loads[6].wait()
     others = pl.ds(1, groups - 1)
     pltpu.make_async_copy(incoming.at[others], incoming.at[others], recv_sem.at[0]).wait()
 
@@ -94,13 +95,12 @@
     gate_act = jnp.dot(x, gate[...], preferred_element_type=jnp.float32)
     up_act = jnp.dot(x, up[...], preferred_element_type=jnp.float32)
     hidden = (gate_act / (1.0 + jnp.exp(-gate_act)) * up_act).astype(jnp.bfloat16)
-    loads[6].wait()
 
     def block_of(q, side):
         columns = pl.ds(pl.multiple_of((lax.rem(row + q, rows) * 2 + side) * part, part), part)
         return jnp.dot(hidden, down[:, columns], preferred_element_type=jnp.float32)
 
-    def give(place, q):
+    def give(place, q, low, high):
         def to(step):
             target = far_first(step)
 
@@ -114,12 +114,14 @@
                 pl.when(target != ep)(copy)
             else:
                 copy()
-        each(0, groups, to)
+        each(low, high, to)
+
+    half = groups // 2
 
     for q in range(2, shares):
         block = block_of(q // 2, lax.rem(core + q, 2))
         partial[(q - 1) * groups:q * groups] = block.reshape(groups, CAP, part)
-        give(q - 1, q)
+        give(q - 1, q, 0, half)
 
     lent[...] = block_of(0, 1 - core)
     lend = pltpu.make_async_remote_copy(
@@ -127,9 +129,11 @@
         device_id=(ep, toward(1)), device_id_type=MESH)
     lend.start()
     block = block_of(0, core)
+    for q in range(2, shares):
+        give(q - 1, q, half, groups)
     lend.wait_recv()
     partial[0:groups] = (block + borrowed[...]).reshape(groups, CAP, part)
-    give(0, 0)
+    give(0, 0, 0, groups)
     arrived[0] = partial[0]
 
     rest = pl.ds(1, groups * (shares - 1) - 1)

time: 19.9 us -> 19.8 us (level)
  no operation moved by 1% of the time
where the time goes in v5:
time: 19.8 us; the launch traced here: 19.6 us
  Pallas kernels  18.3 us (92%)
  local copies, waits for them, and re-layouts  1.3 us (7%)
    pallas_call x1, Pallas kernels, local(): pl.pallas_call(functools.partial(kernel, groups, shares), out_shape=jax.S...  18.3 us
    unnamed x1, local copies, waits for them, and re-layouts  1.3 us

profile of v5, /device:TPU:0, one launch (start us, length us, event | category | flops | bytes accessed | tf_op | source)
XLA Modules:
  0.0 19.6 jit_solution(9510665369897752128)
XLA Ops:
  0.0 18.3 %experts.1 = bf16[16,256]{1,0:T(8,128)(2,1)} custom-call(bf16[16,1024]{1,0:T(8,128)(2,1)} %tokens_hbm.1, f32[1,1024]{1,0:T(1,128)} %bitcast.3, s32[2,16]{1,0:T(2,128)} %bitcast.4, f32[2,16]{1,0:T(2,128)} %bitcast.5, bf16[1,1024,896]{2,1,0:T(8,128)(2,1)} %gate_hbm.1, bf16[1,1024,896]{2,1,0:T(8,128)(2,1)} %up_hbm.1, bf16[1,896,1024]{2,1,0:T(8,128)(2,1)} %down_hbm.1), custom_call_target="tpu_custom_call" | custom-call | tf_op jit(solution)/shard_map/experts/pallas_call | solution.py:160
  18.3 1.3 %copy.9 = bf16[16,256]{1,0:T(8,128)(2,1)} copy(bf16[16,256]{1,0:T(8,128)(2,1)} %experts.1) | data formatting | bytes 16384

commit v6 on v5

--- a/solution.py
+++ b/solution.py
@@ -108,7 +108,7 @@
                 d = lax.rem(ep - target + groups, groups)
                 pltpu.make_async_remote_copy(
                     src_ref=partial.at[place * groups + d], dst_ref=arrived.at[place * groups + d],
-                    send_sem=send_sem.at[1], recv_sem=recv_sem.at[1],
+                    send_sem=send_sem.at[1], recv_sem=recv_sem.at[3 if place == 0 else 1],
                     device_id=(target, toward(q)), device_id_type=MESH).start()
             if q == 0:
                 pl.when(target != ep)(copy)
@@ -136,13 +136,19 @@
     give(0, 0, 0, groups)
     arrived[0] = partial[0]
 
+    def mix(blocks):
+        return jnp.dot(weight, blocks.reshape(slots, part), precision=lax.Precision.HIGHEST,
+                       preferred_element_type=jnp.float32)
+
     rest = pl.ds(1, groups * (shares - 1) - 1)
-    pltpu.make_async_copy(arrived.at[rest], arrived.at[rest], recv_sem.at[1]).wait()
-    total = arrived[0:groups]
-    for q in range(1, shares - 1):
+    far = pl.ds(groups, groups * (shares - 2))
+    pltpu.make_async_copy(arrived.at[others], arrived.at[others], recv_sem.at[3]).wait()
+    out = mix(arrived[0:groups])
+    pltpu.make_async_copy(arrived.at[far], arrived.at[far], recv_sem.at[1]).wait()
+    total = arrived[groups:2 * groups]
+    for q in range(2, shares - 1):
         total = total + arrived[q * groups:(q + 1) * groups]
-    out = jnp.dot(weight, total.reshape(slots, part), precision=lax.Precision.HIGHEST,
-                  preferred_element_type=jnp.float32)
+    out = out + mix(total)
     mixed[...] = out.astype(mixed.dtype)
     pltpu.make_async_copy(outgoing.at[others], outgoing.at[others], send_sem.at[0]).wait()
     pltpu.make_async_copy(partial.at[rest], partial.at[rest], send_sem.at[1]).wait()
@@ -177,8 +183,8 @@
                 pltpu.VMEM((groups * (shares - 1), CAP, part), jnp.float32),
                 pltpu.VMEM((groups * (shares - 1), CAP, part), jnp.float32),
                 pltpu.SemaphoreType.DMA((7,)),
-                pltpu.SemaphoreType.DMA((3,)),
-                pltpu.SemaphoreType.DMA((3,)),
+                pltpu.SemaphoreType.DMA((4,)),
+                pltpu.SemaphoreType.DMA((4,)),
             ],
             compiler_params=pltpu.CompilerParams(collective_id=0, has_side_effects=True,
                                                  vmem_limit_bytes=67043328),

time: 19.8 us -> 19.9 us (level)
  no operation moved by 1% of the time
where the time goes in v6:
time: 19.9 us; the launch traced here: 19.7 us
  Pallas kernels  18.4 us (92%)
  local copies, waits for them, and re-layouts  1.3 us (7%)
    pallas_call x1, Pallas kernels, local(): pl.pallas_call(functools.partial(kernel, groups, shares), out_shape=jax.S...  18.4 us
    unnamed x1, local copies, waits for them, and re-layouts  1.3 us

profile of v6, /device:TPU:0, one launch (start us, length us, event | category | flops | bytes accessed | tf_op | source)
XLA Modules:
  0.0 19.7 jit_solution(13478721151996147528)
XLA Ops:
  0.0 18.4 %experts.1 = bf16[16,256]{1,0:T(8,128)(2,1)} custom-call(bf16[16,1024]{1,0:T(8,128)(2,1)} %tokens_hbm.1, f32[1,1024]{1,0:T(1,128)} %bitcast.3, s32[2,16]{1,0:T(2,128)} %bitcast.4, f32[2,16]{1,0:T(2,128)} %bitcast.5, bf16[1,1024,896]{2,1,0:T(8,128)(2,1)} %gate_hbm.1, bf16[1,1024,896]{2,1,0:T(8,128)(2,1)} %up_hbm.1, bf16[1,896,1024]{2,1,0:T(8,128)(2,1)} %down_hbm.1), custom_call_target="tpu_custom_call" | custom-call | tf_op jit(solution)/shard_map/experts/pallas_call | solution.py:166
  18.4 1.3 %copy.9 = bf16[16,256]{1,0:T(8,128)(2,1)} copy(bf16[16,256]{1,0:T(8,128)(2,1)} %experts.1) | data formatting | bytes 16384
